TPU v7x, 32 devices: a whole 2x2x4 slice. The times are simulated.
32 devices in a mesh: sp: 8 (over z, x), tp: 4 (over y, core).
Axes of the slice: x: 2, y: 2, z: 4, core: 2. Of those that a mesh axis runs over, the one named last changes fastest.
Arguments:
- hidden_states: bfloat16 [6144, 4096], P('sp'), may hold values from -60 to 60
- w_conv_b: bfloat16 [4096, 2048], P(None, 'tp'), may hold values from -0.09375 to 0.09375
- w_conv_c: bfloat16 [4096, 2048], P(None, 'tp'), may hold values from -0.09375 to 0.09375
- w_conv_h: bfloat16 [4096, 2048], P(None, 'tp'), may hold values from -0.09375 to 0.09375
- conv_taps: bfloat16 [3, 2048], P(None, 'tp'), may hold values from -3.5 to 3.5
- w_query: bfloat16 [4096, 2048], P(None, 'tp'), may hold values from -0.15625 to 0.15625
- w_key: bfloat16 [4096, 2048], P(None, 'tp'), may hold values from -0.09375 to 0.09375
- w_value: bfloat16 [4096, 2048], P(None, 'tp'), may hold values from -0.09375 to 0.09375
- lambdas: float32 [16], P('tp'), may hold values from 0.3 to 0.8
- head_gain: bfloat16 [128], replicated, may hold values from 0.099609375 to 1.8984375
- w_out_conv: bfloat16 [2048, 4096], P('tp'), may hold values from -1 to 1
- w_out_attn: bfloat16 [2048, 4096], P('tp'), may hold values from -1 to 1
- out_gain: bfloat16 [4096], replicated, may hold values from 0.099609375 to 1.8984375
Outputs:
- mixed: bfloat16 [6144, 4096], P('sp', 'tp')
All inputs are finite; a program needn't handle non-finite values.
Results may differ from a plain program's by a relative error of at most 0.023.
Values may be sent and summed in bfloat16 or wider, within the bound.
A program may use at most 192 MiB of HBM per device.

v0:
```python
import jax
import jax.numpy as jnp
from jax import lax
from jax.sharding import PartitionSpec as P

D = 4096
QK = 64
TAPS = 3
VD = 128
NEG_LARGE = -1e30


def passed_along(block, axis, distance):
    devices = range(lax.axis_size(axis))
    route = [(i - distance, i) for i in devices if i - distance in devices]
    return lax.ppermute(block, axis, route)


def rotate(values, positions):
    inverse = 1.0 / 10000.0 ** (jnp.arange(0, QK, 2, dtype=jnp.float32) / QK)
    angles = positions[:, None] * inverse[None, :]
    angles = jnp.concatenate([angles, angles], axis=-1)
    cosine = jnp.cos(angles)[:, None, None, :]
    sine = jnp.sin(angles)[:, None, None, :]
    first_half, second_half = jnp.split(values, 2, axis=-1)
    return values * cosine + jnp.concatenate([-second_half, first_half], axis=-1) * sine


def per_device(
    hidden_states,
    w_conv_b,
    w_conv_c,
    w_conv_h,
    conv_taps,
    w_query,
    w_key,
    w_value,
    lambdas,
    head_gain,
    w_out_conv,
    w_out_attn,
    out_gain,
):
    tok_rows = hidden_states.shape[0]
    head_count = w_value.shape[1] // VD
    channels = w_conv_b.shape[1]
    offset = lax.axis_index("sp") * tok_rows
    query_pos = offset + jnp.arange(tok_rows, dtype=jnp.int32)
    positions = query_pos.astype(jnp.float32)

    def project(weight):
        return jnp.dot(hidden_states, weight, preferred_element_type=jnp.float32).astype(
            jnp.bfloat16
        )

    key_rot = rotate(
        project(w_key).reshape(tok_rows, head_count, 2, QK).astype(jnp.float32), positions
    ).astype(jnp.bfloat16)
    values = project(w_value)
    query_rot = rotate(
        project(w_query).reshape(tok_rows, head_count, 2, QK).astype(jnp.float32), positions
    ).astype(jnp.bfloat16)
    scale = QK ** (-0.5)

    def attend(state, keys_blk, vals_blk, first_pos):
        running_max, running_sum, numer = state
        scores = (
            jnp.einsum("qhcd,khcd->hcqk", query_rot, keys_blk, preferred_element_type=jnp.float32)
            * scale
        )
        key_pos = first_pos + jnp.arange(keys_blk.shape[0], dtype=jnp.int32)
        visible = (key_pos[None, :] <= query_pos[:, None])[None, None]
        scores = jnp.where(visible, scores, NEG_LARGE)
        new_max = jnp.maximum(running_max, jnp.max(scores, axis=-1))
        weights = jnp.where(visible, jnp.exp(scores - new_max[..., None]), 0.0)
        factor = jnp.exp(running_max - new_max)
        running_sum = running_sum * factor + jnp.sum(weights, axis=-1)
        numer = numer * factor[..., None] + jnp.einsum(
            "hcqk,khe->hcqe",
            weights.astype(jnp.bfloat16),
            vals_blk,
            preferred_element_type=jnp.float32,
        )
        return (new_max, running_sum, numer)

    initial = (
        jnp.full((head_count, 2, tok_rows), NEG_LARGE, jnp.float32),
        jnp.zeros((head_count, 2, tok_rows), jnp.float32),
        jnp.zeros((head_count, 2, tok_rows, VD), jnp.float32),
    )
    packed_keys = key_rot.reshape(tok_rows, head_count * 2 * QK)
    key_piece = lax.all_gather(packed_keys, "sp", axis=0, tiled=True)
    value_piece = lax.all_gather(values, "sp", axis=0, tiled=True)
    count = key_piece.shape[0]
    block = 512

    def one_block(index, state):
        first = index * block
        keys_blk = lax.dynamic_slice_in_dim(key_piece, first, block, 0).reshape(
            block, head_count, 2, QK
        )
        vals_blk = lax.dynamic_slice_in_dim(value_piece, first, block, 0).reshape(
            block, head_count, VD
        )
        return attend(state, keys_blk, vals_blk, first)

    def work(state):
        return lax.fori_loop(0, count // block, one_block, state)

    running_max, running_sum, numer = lax.cond(
        jnp.int32(0) <= offset + tok_rows - 1, work, lambda state: state, initial
    )
    u_b = project(w_conv_b)
    u_c = project(w_conv_c)
    u_h = project(w_conv_h)
    gated = u_c.astype(jnp.float32) * u_h.astype(jnp.float32)
    rim_rows = passed_along(gated[tok_rows - (TAPS - 1) :], "sp", 1)
    padded = jnp.concatenate([rim_rows, gated], axis=0)
    taps_f = conv_taps.astype(jnp.float32)
    convolved = jnp.zeros((tok_rows, channels), jnp.float32)
    for tap in range(TAPS):
        convolved = convolved + taps_f[tap][None, :] * padded[tap : tap + tok_rows]
    conv_out = (u_b.astype(jnp.float32) * convolved).astype(jnp.bfloat16)
    diff = (
        numer[:, 0] / running_sum[:, 0, :, None]
        - lambdas[:, None, None] * numer[:, 1] / running_sum[:, 1, :, None]
    )
    normed = (
        diff
        * lax.rsqrt(jnp.mean(diff * diff, axis=-1, keepdims=True) + 1e-05)
        * head_gain.astype(jnp.float32)[None, None, :]
    )
    attn_out = normed.astype(jnp.bfloat16).transpose(1, 0, 2).reshape(tok_rows, head_count * VD)
    gain_f = out_gain.astype(jnp.float32)
    partial_value = jnp.dot(conv_out, w_out_conv, preferred_element_type=jnp.float32) + jnp.dot(
        attn_out, w_out_attn, preferred_element_type=jnp.float32
    )
    summed = lax.psum_scatter(
        partial_value.astype(jnp.bfloat16), "tp", scatter_dimension=1, tiled=True
    )
    mix_f = summed.astype(jnp.float32)
    width = mix_f.shape[1]
    total_sum, total_squares = lax.psum(
        (jnp.sum(mix_f, axis=-1), jnp.sum(mix_f * mix_f, axis=-1)), "tp"
    )
    mean_value = (total_sum / D)[:, None]
    variance = (total_squares / D)[:, None] - mean_value * mean_value
    own_gain = lax.dynamic_slice_in_dim(gain_f, lax.axis_index("tp") * width, width, 0)
    return ((mix_f - mean_value) * lax.rsqrt(variance + 1e-05) * own_gain[None, :]).astype(
        jnp.bfloat16
    )


def solution(mesh):
    return jax.shard_map(
        per_device,
        mesh=mesh,
        in_specs=(
            P("sp", None),
            P(None, "tp"),
            P(None, "tp"),
            P(None, "tp"),
            P(None, "tp"),
            P(None, "tp"),
            P(None, "tp"),
            P(None, "tp"),
            P("tp"),
            P(),
            P("tp", None),
            P("tp", None),
            P(),
        ),
        out_specs=P("sp", "tp"),
        check_vma=False,
    )
```

profile of v0, /device:TPU:0, one launch (start us, length us, event | category | flops | bytes accessed | tf_op | source)
XLA Modules:
  0.0 625.5 jit_solution(7716799668903363379)
XLA Ops:
  6.6 7.6 %convolution_convert_fusion.1 = bf16[768,512]{0,1:T(8,128)(2,1)S(1)} fusion(bf16[768,4096]{1,0:T(8,128)(2,1)} %param.17, bf16[4096,512]{1,0:T(8,128)(2,1)} %param.22), kind=kOutput, calls=%fused_computation.57 | convolution fusion | flops 3221618688 | bytes 11272192 | tf_op jit(solution)/shard_map/dot_general | solution.py:52
  24.7 8.3 %convolution_convert_fusion = bf16[768,512]{1,0:T(8,128)(2,1)} fusion(bf16[768,4096]{1,0:T(8,128)(2,1)} %param.17, bf16[4096,512]{1,0:T(8,128)(2,1)} %param.24), kind=kOutput, calls=%fused_computation.56 | convolution fusion | flops 3221618688 | bytes 11272192 | tf_op jit(solution)/shard_map/dot_general | solution.py:52
  33.3 8.4 %convolution_convert_fusion.3 = bf16[768,512]{1,0:T(8,128)(2,1)S(1)} fusion(bf16[768,4096]{1,0:T(8,128)(2,1)} %param.17, bf16[4096,512]{1,0:T(8,128)(2,1)} %param.20), kind=kOutput, calls=%fused_computation.60 | convolution fusion | flops 3221618688 | bytes 11272192 | tf_op jit(solution)/shard_map/dot_general | solution.py:52
  53.2 15.1 %fusion.33 = f32[768,4096]{1,0:T(8,128)} fusion(bf16[512,4096]{1,0:T(8,128)(2,1)} %param.27, f32[2,512]{1,0:T(2,128)S(1)} %collective-permute-done, f32[768,512]{1,0:T(8,128)} %copy-done.2, bf16[768,4096]{1,0:T(8,128)(2,1)} %param.17, bf16[4096,512]{1,0:T(8,128)(2,1)} %param.18, f32[512]{0:T(512)S(1)} %bitcast.103, f32[512]{0:T(512)S(1)} %bitcast.102, ...), kind=kOutput, calls=%fused_computation.65 | convolution fusion | flops 6446776320 | bytes 28846080 | tf_op jit(solution)/shard_map/dot_general | solution.py:135
  68.3 57.8 %all-gather.3.cloned.1.call-done = bf16[6144,512]{0,1:T(8,128)(2,1)} async-done(((bf16[768,512]{0,1:T(8,128)(2,1)}), bf16[6144,512]{0,1:T(8,128)(2,1)}) %all-gather.3.cloned.1.call-update) | async-done | bytes 6291472 | tf_op jit(solution)/shard_map/all_gather | solution.py:92
  126.0 99.4 %all-gather.5.cloned.1.call-done = bf16[6144,512]{1,0:T(8,128)(2,1)} async-done(((bf16[768,512]{1,0:T(8,128)(2,1)}), bf16[6144,512]{1,0:T(8,128)(2,1)}) %all-gather.5.cloned.1.call-update) | async-done | bytes 6291472 | tf_op jit(solution)/shard_map/all_gather | solution.py:93
  225.5 312.6 %conditional.1 = (f32[4,2,768]{2,1,0:T(2,128)}, f32[4,2,768,128]{3,2,1,0:T(8,128)}) conditional(s32[]{:T(128)} %convert_element_type.98, () %tuple.27, (s32[]{:T(128)}, s32[768]{0:T(1024)S(1)}, bf16[6144,512]{0,1:T(8,128)(2,1)}, bf16[768,4,2,64]{0,3,2,1:T(8,128)(2,1)S(1)}, bf16[6144,512]{1,0:T(8,128)(2,1)}) %tuple.28), branch_computations={%region_0.0_spmd, %region_1.6_spmd} | conditional | flops 1251638528 | bytes 51000628 | solution.py:110
  225.5 312.6 %while.17 = (s32[]{:T(128)}, f32[4,2,768]{2,1,0:T(2,128)S(1)}, f32[4,2,768]{2,1,0:T(2,128)}, f32[4,2,768,128]{3,2,1,0:T(8,128)}, s32[768]{0:T(1024)S(1)}, /*inde...) while((s32[]{:T(128)}, f32[4,2,768]{2,1,0:T(2,128)S(1)}, ...), condition=%wide.region_5.5_spmd.clone, body=%wide.region_2.4_spmd.clone.sunk | while | flops 1251637760 | bytes 50994360 | solution.py:108
  241.9 8.5 %fusion.75 = f32[4,2,768,128]{3,2,1,0:T(8,128)} fusion(f32[4,2,768,128]{3,2,1,0:T(8,128)} %get-tuple-element.310, bf16[512,4,128,1]{0,2,3,1:T(8,128)(2,1)S(1)} %bitcast.93, f32[4,2,512,768]{3,2,1,0:T(8,128)} %get-tuple-element.292, f32[4,2,768]{2,1,0:T(2,128)S(1)} %fusion.72, pred[768,512]{0,1:T(8,128)(4,1)S(1)} %broadcast_compare_fusion.2, ...), kind=kOutput, calls=%fused_computation.8.clone.1 | convolution fusion | flops 823394304 | bytes 19841024 | tf_op jit(solution)/shard_map/cond/branch_1_fun/while/body/eval_jaxpr/hcqk,khe->hcqe/dot_general | solution.py:78
  251.8 6.6 %fusion.71 = (f32[4,2,768]{2,1,0:T(2,128)S(1)}, f32[4,2,512,768]{3,2,1,0:T(8,128)}) fusion(pred[768,512]{0,1:T(8,128)(4,1)S(1)} %broadcast_compare_fusion.2, bf16[512,4,2,64]{0,3,2,1:T(8,128)(2,1)S(1)} %bitcast.92, bf16[768,4,2,64]{0,3,2,1:T(8,128)(2,1)S(1)} %get-tuple-element.325), kind=kOutput, calls=%fused_computation.2.clone.1 | convolution fusion | flops 412084224 | bytes 14311424 | tf_op jit(solution)/shard_map/cond/branch_1_fun/while/body/eval_jaxpr/qhcd,khcd->hcqk/dot_general | solution.py:68
  267.6 9.0 %fusion.75 = f32[4,2,768,128]{3,2,1,0:T(8,128)} fusion(f32[4,2,768,128]{3,2,1,0:T(8,128)} %get-tuple-element.310, bf16[512,4,128,1]{0,2,3,1:T(8,128)(2,1)S(1)} %bitcast.93, f32[4,2,512,768]{3,2,1,0:T(8,128)} %get-tuple-element.292, f32[4,2,768]{2,1,0:T(2,128)S(1)} %fusion.72, pred[768,512]{0,1:T(8,128)(4,1)S(1)} %broadcast_compare_fusion.2, ...), kind=kOutput, calls=%fused_computation.8.clone.1 | convolution fusion | flops 823394304 | bytes 19841024 | tf_op jit(solution)/shard_map/cond/branch_1_fun/while/body/eval_jaxpr/hcqk,khe->hcqe/dot_general | solution.py:78
  278.0 6.6 %fusion.71 = (f32[4,2,768]{2,1,0:T(2,128)S(1)}, f32[4,2,512,768]{3,2,1,0:T(8,128)}) fusion(pred[768,512]{0,1:T(8,128)(4,1)S(1)} %broadcast_compare_fusion.2, bf16[512,4,2,64]{0,3,2,1:T(8,128)(2,1)S(1)} %bitcast.92, bf16[768,4,2,64]{0,3,2,1:T(8,128)(2,1)S(1)} %get-tuple-element.325), kind=kOutput, calls=%fused_computation.2.clone.1 | convolution fusion | flops 412084224 | bytes 14311424 | tf_op jit(solution)/shard_map/cond/branch_1_fun/while/body/eval_jaxpr/qhcd,khcd->hcqk/dot_general | solution.py:68
  293.8 9.0 %fusion.75 = f32[4,2,768,128]{3,2,1,0:T(8,128)} fusion(f32[4,2,768,128]{3,2,1,0:T(8,128)} %get-tuple-element.310, bf16[512,4,128,1]{0,2,3,1:T(8,128)(2,1)S(1)} %bitcast.93, f32[4,2,512,768]{3,2,1,0:T(8,128)} %get-tuple-element.292, f32[4,2,768]{2,1,0:T(2,128)S(1)} %fusion.72, pred[768,512]{0,1:T(8,128)(4,1)S(1)} %broadcast_compare_fusion.2, ...), kind=kOutput, calls=%fused_computation.8.clone.1 | convolution fusion | flops 823394304 | bytes 19841024 | tf_op jit(solution)/shard_map/cond/branch_1_fun/while/body/eval_jaxpr/hcqk,khe->hcqe/dot_general | solution.py:78
  319.9 9.0 %fusion.75 = f32[4,2,768,128]{3,2,1,0:T(8,128)} fusion(f32[4,2,768,128]{3,2,1,0:T(8,128)} %get-tuple-element.310, bf16[512,4,128,1]{0,2,3,1:T(8,128)(2,1)S(1)} %bitcast.93, f32[4,2,512,768]{3,2,1,0:T(8,128)} %get-tuple-element.292, f32[4,2,768]{2,1,0:T(2,128)S(1)} %fusion.72, pred[768,512]{0,1:T(8,128)(4,1)S(1)} %broadcast_compare_fusion.2, ...), kind=kOutput, calls=%fused_computation.8.clone.1 | convolution fusion | flops 823394304 | bytes 19841024 | tf_op jit(solution)/shard_map/cond/branch_1_fun/while/body/eval_jaxpr/hcqk,khe->hcqe/dot_general | solution.py:78
  330.3 6.6 %fusion.71 = (f32[4,2,768]{2,1,0:T(2,128)S(1)}, f32[4,2,512,768]{3,2,1,0:T(8,128)}) fusion(pred[768,512]{0,1:T(8,128)(4,1)S(1)} %broadcast_compare_fusion.2, bf16[512,4,2,64]{0,3,2,1:T(8,128)(2,1)S(1)} %bitcast.92, bf16[768,4,2,64]{0,3,2,1:T(8,128)(2,1)S(1)} %get-tuple-element.325), kind=kOutput, calls=%fused_computation.2.clone.1 | convolution fusion | flops 412084224 | bytes 14311424 | tf_op jit(solution)/shard_map/cond/branch_1_fun/while/body/eval_jaxpr/qhcd,khcd->hcqk/dot_general | solution.py:68
  346.1 9.0 %fusion.75 = f32[4,2,768,128]{3,2,1,0:T(8,128)} fusion(f32[4,2,768,128]{3,2,1,0:T(8,128)} %get-tuple-element.310, bf16[512,4,128,1]{0,2,3,1:T(8,128)(2,1)S(1)} %bitcast.93, f32[4,2,512,768]{3,2,1,0:T(8,128)} %get-tuple-element.292, f32[4,2,768]{2,1,0:T(2,128)S(1)} %fusion.72, pred[768,512]{0,1:T(8,128)(4,1)S(1)} %broadcast_compare_fusion.2, ...), kind=kOutput, calls=%fused_computation.8.clone.1 | convolution fusion | flops 823394304 | bytes 19841024 | tf_op jit(solution)/shard_map/cond/branch_1_fun/while/body/eval_jaxpr/hcqk,khe->hcqe/dot_general | solution.py:78
  356.4 6.6 %fusion.71 = (f32[4,2,768]{2,1,0:T(2,128)S(1)}, f32[4,2,512,768]{3,2,1,0:T(8,128)}) fusion(pred[768,512]{0,1:T(8,128)(4,1)S(1)} %broadcast_compare_fusion.2, bf16[512,4,2,64]{0,3,2,1:T(8,128)(2,1)S(1)} %bitcast.92, bf16[768,4,2,64]{0,3,2,1:T(8,128)(2,1)S(1)} %get-tuple-element.325), kind=kOutput, calls=%fused_computation.2.clone.1 | convolution fusion | flops 412084224 | bytes 14311424 | tf_op jit(solution)/shard_map/cond/branch_1_fun/while/body/eval_jaxpr/qhcd,khcd->hcqk/dot_general | solution.py:68
  372.2 9.0 %fusion.75 = f32[4,2,768,128]{3,2,1,0:T(8,128)} fusion(f32[4,2,768,128]{3,2,1,0:T(8,128)} %get-tuple-element.310, bf16[512,4,128,1]{0,2,3,1:T(8,128)(2,1)S(1)} %bitcast.93, f32[4,2,512,768]{3,2,1,0:T(8,128)} %get-tuple-element.292, f32[4,2,768]{2,1,0:T(2,128)S(1)} %fusion.72, pred[768,512]{0,1:T(8,128)(4,1)S(1)} %broadcast_compare_fusion.2, ...), kind=kOutput, calls=%fused_computation.8.clone.1 | convolution fusion | flops 823394304 | bytes 19841024 | tf_op jit(solution)/shard_map/cond/branch_1_fun/while/body/eval_jaxpr/hcqk,khe->hcqe/dot_general | solution.py:78
  382.6 6.6 %fusion.71 = (f32[4,2,768]{2,1,0:T(2,128)S(1)}, f32[4,2,512,768]{3,2,1,0:T(8,128)}) fusion(pred[768,512]{0,1:T(8,128)(4,1)S(1)} %broadcast_compare_fusion.2, bf16[512,4,2,64]{0,3,2,1:T(8,128)(2,1)S(1)} %bitcast.92, bf16[768,4,2,64]{0,3,2,1:T(8,128)(2,1)S(1)} %get-tuple-element.325), kind=kOutput, calls=%fused_computation.2.clone.1 | convolution fusion | flops 412084224 | bytes 14311424 | tf_op jit(solution)/shard_map/cond/branch_1_fun/while/body/eval_jaxpr/qhcd,khcd->hcqk/dot_general | solution.py:68
  398.3 9.0 %fusion.75 = f32[4,2,768,128]{3,2,1,0:T(8,128)} fusion(f32[4,2,768,128]{3,2,1,0:T(8,128)} %get-tuple-element.310, bf16[512,4,128,1]{0,2,3,1:T(8,128)(2,1)S(1)} %bitcast.93, f32[4,2,512,768]{3,2,1,0:T(8,128)} %get-tuple-element.292, f32[4,2,768]{2,1,0:T(2,128)S(1)} %fusion.72, pred[768,512]{0,1:T(8,128)(4,1)S(1)} %broadcast_compare_fusion.2, ...), kind=kOutput, calls=%fused_computation.8.clone.1 | convolution fusion | flops 823394304 | bytes 19841024 | tf_op jit(solution)/shard_map/cond/branch_1_fun/while/body/eval_jaxpr/hcqk,khe->hcqe/dot_general | solution.py:78
  408.7 6.6 %fusion.71 = (f32[4,2,768]{2,1,0:T(2,128)S(1)}, f32[4,2,512,768]{3,2,1,0:T(8,128)}) fusion(pred[768,512]{0,1:T(8,128)(4,1)S(1)} %broadcast_compare_fusion.2, bf16[512,4,2,64]{0,3,2,1:T(8,128)(2,1)S(1)} %bitcast.92, bf16[768,4,2,64]{0,3,2,1:T(8,128)(2,1)S(1)} %get-tuple-element.325), kind=kOutput, calls=%fused_computation.2.clone.1 | convolution fusion | flops 412084224 | bytes 14311424 | tf_op jit(solution)/shard_map/cond/branch_1_fun/while/body/eval_jaxpr/qhcd,khcd->hcqk/dot_general | solution.py:68
  424.5 9.0 %fusion.75 = f32[4,2,768,128]{3,2,1,0:T(8,128)} fusion(f32[4,2,768,128]{3,2,1,0:T(8,128)} %get-tuple-element.310, bf16[512,4,128,1]{0,2,3,1:T(8,128)(2,1)S(1)} %bitcast.93, f32[4,2,512,768]{3,2,1,0:T(8,128)} %get-tuple-element.292, f32[4,2,768]{2,1,0:T(2,128)S(1)} %fusion.72, pred[768,512]{0,1:T(8,128)(4,1)S(1)} %broadcast_compare_fusion.2, ...), kind=kOutput, calls=%fused_computation.8.clone.1 | convolution fusion | flops 823394304 | bytes 19841024 | tf_op jit(solution)/shard_map/cond/branch_1_fun/while/body/eval_jaxpr/hcqk,khe->hcqe/dot_general | solution.py:78
  434.9 6.6 %fusion.71 = (f32[4,2,768]{2,1,0:T(2,128)S(1)}, f32[4,2,512,768]{3,2,1,0:T(8,128)}) fusion(pred[768,512]{0,1:T(8,128)(4,1)S(1)} %broadcast_compare_fusion.2, bf16[512,4,2,64]{0,3,2,1:T(8,128)(2,1)S(1)} %bitcast.92, bf16[768,4,2,64]{0,3,2,1:T(8,128)(2,1)S(1)} %get-tuple-element.325), kind=kOutput, calls=%fused_computation.2.clone.1 | convolution fusion | flops 412084224 | bytes 14311424 | tf_op jit(solution)/shard_map/cond/branch_1_fun/while/body/eval_jaxpr/qhcd,khcd->hcqk/dot_general | solution.py:68
  450.6 9.0 %fusion.75 = f32[4,2,768,128]{3,2,1,0:T(8,128)} fusion(f32[4,2,768,128]{3,2,1,0:T(8,128)} %get-tuple-element.310, bf16[512,4,128,1]{0,2,3,1:T(8,128)(2,1)S(1)} %bitcast.93, f32[4,2,512,768]{3,2,1,0:T(8,128)} %get-tuple-element.292, f32[4,2,768]{2,1,0:T(2,128)S(1)} %fusion.72, pred[768,512]{0,1:T(8,128)(4,1)S(1)} %broadcast_compare_fusion.2, ...), kind=kOutput, calls=%fused_computation.8.clone.1 | convolution fusion | flops 823394304 | bytes 19841024 | tf_op jit(solution)/shard_map/cond/branch_1_fun/while/body/eval_jaxpr/hcqk,khe->hcqe/dot_general | solution.py:78
  461.0 6.6 %fusion.71 = (f32[4,2,768]{2,1,0:T(2,128)S(1)}, f32[4,2,512,768]{3,2,1,0:T(8,128)}) fusion(pred[768,512]{0,1:T(8,128)(4,1)S(1)} %broadcast_compare_fusion.2, bf16[512,4,2,64]{0,3,2,1:T(8,128)(2,1)S(1)} %bitcast.92, bf16[768,4,2,64]{0,3,2,1:T(8,128)(2,1)S(1)} %get-tuple-element.325), kind=kOutput, calls=%fused_computation.2.clone.1 | convolution fusion | flops 412084224 | bytes 14311424 | tf_op jit(solution)/shard_map/cond/branch_1_fun/while/body/eval_jaxpr/qhcd,khcd->hcqk/dot_general | solution.py:68
  476.8 9.0 %fusion.75 = f32[4,2,768,128]{3,2,1,0:T(8,128)} fusion(f32[4,2,768,128]{3,2,1,0:T(8,128)} %get-tuple-element.310, bf16[512,4,128,1]{0,2,3,1:T(8,128)(2,1)S(1)} %bitcast.93, f32[4,2,512,768]{3,2,1,0:T(8,128)} %get-tuple-element.292, f32[4,2,768]{2,1,0:T(2,128)S(1)} %fusion.72, pred[768,512]{0,1:T(8,128)(4,1)S(1)} %broadcast_compare_fusion.2, ...), kind=kOutput, calls=%fused_computation.8.clone.1 | convolution fusion | flops 823394304 | bytes 19841024 | tf_op jit(solution)/shard_map/cond/branch_1_fun/while/body/eval_jaxpr/hcqk,khe->hcqe/dot_general | solution.py:78
  487.2 6.6 %fusion.71 = (f32[4,2,768]{2,1,0:T(2,128)S(1)}, f32[4,2,512,768]{3,2,1,0:T(8,128)}) fusion(pred[768,512]{0,1:T(8,128)(4,1)S(1)} %broadcast_compare_fusion.2, bf16[512,4,2,64]{0,3,2,1:T(8,128)(2,1)S(1)} %bitcast.92, bf16[768,4,2,64]{0,3,2,1:T(8,128)(2,1)S(1)} %get-tuple-element.325), kind=kOutput, calls=%fused_computation.2.clone.1 | convolution fusion | flops 412084224 | bytes 14311424 | tf_op jit(solution)/shard_map/cond/branch_1_fun/while/body/eval_jaxpr/qhcd,khcd->hcqk/dot_general | solution.py:68
  502.9 9.0 %fusion.75 = f32[4,2,768,128]{3,2,1,0:T(8,128)} fusion(f32[4,2,768,128]{3,2,1,0:T(8,128)} %get-tuple-element.310, bf16[512,4,128,1]{0,2,3,1:T(8,128)(2,1)S(1)} %bitcast.93, f32[4,2,512,768]{3,2,1,0:T(8,128)} %get-tuple-element.292, f32[4,2,768]{2,1,0:T(2,128)S(1)} %fusion.72, pred[768,512]{0,1:T(8,128)(4,1)S(1)} %broadcast_compare_fusion.2, ...), kind=kOutput, calls=%fused_computation.8.clone.1 | convolution fusion | flops 823394304 | bytes 19841024 | tf_op jit(solution)/shard_map/cond/branch_1_fun/while/body/eval_jaxpr/hcqk,khe->hcqe/dot_general | solution.py:78
  513.3 6.6 %fusion.71 = (f32[4,2,768]{2,1,0:T(2,128)S(1)}, f32[4,2,512,768]{3,2,1,0:T(8,128)}) fusion(pred[768,512]{0,1:T(8,128)(4,1)S(1)} %broadcast_compare_fusion.2, bf16[512,4,2,64]{0,3,2,1:T(8,128)(2,1)S(1)} %bitcast.92, bf16[768,4,2,64]{0,3,2,1:T(8,128)(2,1)S(1)} %get-tuple-element.325), kind=kOutput, calls=%fused_computation.2.clone.1 | convolution fusion | flops 412084224 | bytes 14311424 | tf_op jit(solution)/shard_map/cond/branch_1_fun/while/body/eval_jaxpr/qhcd,khcd->hcqk/dot_general | solution.py:68
  529.1 9.0 %fusion.75 = f32[4,2,768,128]{3,2,1,0:T(8,128)} fusion(f32[4,2,768,128]{3,2,1,0:T(8,128)} %get-tuple-element.310, bf16[512,4,128,1]{0,2,3,1:T(8,128)(2,1)S(1)} %bitcast.93, f32[4,2,512,768]{3,2,1,0:T(8,128)} %get-tuple-element.292, f32[4,2,768]{2,1,0:T(2,128)S(1)} %fusion.72, pred[768,512]{0,1:T(8,128)(4,1)S(1)} %broadcast_compare_fusion.2, ...), kind=kOutput, calls=%fused_computation.8.clone.1 | convolution fusion | flops 823394304 | bytes 19841024 | tf_op jit(solution)/shard_map/cond/branch_1_fun/while/body/eval_jaxpr/hcqk,khe->hcqe/dot_general | solution.py:78
  543.6 8.2 %add_convert_fusion = bf16[768,4096]{1,0:T(8,128)(2,1)} fusion(f32[768,4096]{1,0:T(8,128)} %fusion.33, bf16[768,512]{0,1:T(8,128)(2,1)S(1)} %bitcast.98, bf16[512,4096]{1,0:T(8,128)(2,1)S(1)} %copy-done.6), kind=kOutput, calls=%fused_computation.22 | convolution fusion | flops 3227516928 | bytes 23855104 | tf_op jit(solution)/shard_map/dot_general | solution.py:135
  552.5 55.6 %reduce-scatter.2.cloned.1.call-done = bf16[768,1024]{1,0:T(8,128)(2,1)} async-done(((bf16[768,4096]{1,0:T(8,128)(2,1)}), bf16[768,1024]{1,0:T(8,128)(2,1)}) %reduce-scatter.2.cloned.1.call-update) | async-done | bytes 1572880 | tf_op jit(solution)/shard_map/reduce_scatter | solution.py:138
  (165 shorter events, 178.2 us)
Async XLA Ops:
  6.5 119.5 %all-gather.3.cloned.1.call-start = ((), (), s32[]{:S(2)}) async-start(), calls=%async_computation.1 | async-start | bytes 7077888 | tf_op jit(solution)/shard_map/all_gather | solution.py:92
  6.5 9.9 %copy-start.3 = (bf16[768,4096]{1,0:T(8,128)(2,1)S(1)}, bf16[768,4096]{1,0:T(8,128)(2,1)}, u32[]{:S(2)}) copy-start(bf16[768,4096]{1,0:T(8,128)(2,1)} %param.17) | copy-start | bytes 18874372
  6.6 9.9 %copy-start.4 = (bf16[4096,512]{1,0:T(8,128)(2,1)S(1)}, bf16[4096,512]{1,0:T(8,128)(2,1)}, u32[]{:S(2)}) copy-start(bf16[4096,512]{1,0:T(8,128)(2,1)} %param.23) | copy-start | bytes 12582916
  24.7 200.8 %all-gather.5.cloned.1.call-start = ((), (), s32[]{:S(2)}) async-start(), calls=%async_computation.2 | async-start | bytes 7077888 | tf_op jit(solution)/shard_map/all_gather | solution.py:93
  33.0 575.0 %reduce-scatter.2.cloned.1.call-start = ((), (), s32[]{:S(2)}) async-start(), calls=%async_computation.3 | async-start | bytes 7864320 | tf_op jit(solution)/shard_map/reduce_scatter | solution.py:138
  33.3 8.4 %copy-start.5 = (bf16[4096,512]{1,0:T(8,128)(2,1)S(1)}, bf16[4096,512]{1,0:T(8,128)(2,1)}, u32[]{:S(2)}) copy-start(bf16[4096,512]{1,0:T(8,128)(2,1)} %param.19) | copy-start | bytes 12582916
  41.7 10.2 %copy-start = (bf16[3,512]{1,0:T(4,128)(2,1)S(1)}, bf16[3,512]{1,0:T(4,128)(2,1)}, u32[]{:S(2)}) copy-start(bf16[3,512]{1,0:T(4,128)(2,1)} %param.21) | copy-start | bytes 9220
  41.7 10.2 %copy-start.7 = (bf16[128]{0:T(256)(128)(2,1)S(1)}, bf16[128]{0:T(256)(128)(2,1)}, u32[]{:S(2)}) copy-start(bf16[128]{0:T(256)(128)(2,1)} %param.26) | copy-start | bytes 772
  47.2 4.7 copy-start.2
  47.2 5.9 collective-permute-start
  538.9 2.4 copy-start.1
  541.4 2.2 copy-start.6
Sparse Core Ops, SparseCore 0:
  24.8 101.1 all-gather.2
  128.2 97.2 all-gather.4
  551.9 56.0 reduce-scatter.1
where the time goes:
time: 628 us; the launch traced here: 625 us
  matrix products  243 us (39%)
  waiting for transfers between devices  214 us (34%)
  other arithmetic  110 us (18%)
  local copies, waits for them, and re-layouts  34.1 us (5%)
  between operations  13.4 us (2%)
    dot_general x12, matrix products, attend(): jnp.einsum('hcqk,khe->hcqe', weights.astype(jnp.bfloat16), vals_blk, pref...  107 us
    all_gather x1, waiting for transfers between devices, per_device(): value_piece = lax.all_gather(values, 'sp', axis=0, tiled=True)  99.4 us
    dot_general x12, matrix products, attend(): jnp.einsum('qhcd,khcd->hcqk', query_rot, keys_blk, preferred_element_type...  78.7 us
    reduce_sum x12, other arithmetic, attend(): running_sum = running_sum * factor + jnp.sum(weights, axis=-1)  77.7 us
    all_gather x1, waiting for transfers between devices, per_device(): key_piece = lax.all_gather(packed_keys, 'sp', axis=0, tiled=True)  57.8 us
    reduce_scatter x1, waiting for transfers between devices, per_device(): lax.psum_scatter(partial_value.astype(jnp.bfloat16), 'tp', scatter_dimens...  55.6 us
    dot_general x5, matrix products, project(): jnp.dot(hidden_states, weight, preferred_element_type=jnp.float32)  33.6 us
    add x12, other arithmetic, attend(): running_sum = running_sum * factor + jnp.sum(weights, axis=-1)  16 us
  transfers between devices with their start and end apart: 4, of which 4 were waited for; matrix products, arithmetic and copies ran while one was open for 6% of the time, Pallas kernels for 0%

commit v1 on v0

--- a/solution.py
+++ b/solution.py
@@ -89,8 +89,11 @@
         jnp.zeros((head_count, 2, tok_rows, VD), jnp.float32),
     )
     packed_keys = key_rot.reshape(tok_rows, head_count * 2 * QK)
-    key_piece = lax.all_gather(packed_keys, "sp", axis=0, tiled=True)
-    value_piece = lax.all_gather(values, "sp", axis=0, tiled=True)
+    key_piece, value_piece = jnp.split(
+        jax.lax.all_gather(jnp.concatenate([packed_keys, values], 1), "sp", axis=0, tiled=True),
+        [packed_keys.shape[1]],
+        1,
+    )
     count = key_piece.shape[0]
     block = 512
 

time: 628 us -> 593 us (0.944)
  matrix products: 243 us -> 212 us
  waiting for transfers between devices: 214 us -> 201 us
  other arithmetic: 110 us -> 119 us
    dot_general x12, matrix products: 107 us -> 81.2 us  [attend(): jnp.einsum('hcqk,khe->hcqe', weights.astype(jnp.bfloat16), vals_blk, pref...]
    dynamic_slice x12 -> x0, local copies, waits for them, and re-layouts: 12.9 us -> none  [one_block(): lax.dynamic_slice_in_dim(key_piece, first, block, 0)]
    all_gather x2 -> x1, waiting for transfers between devices: 157 us -> 145 us  [per_device(): jax.lax.all_gather(jnp.concatenate([packed_keys, values], 1), 'sp', axis=...]
    split x0 -> x1, local copies, waits for them, and re-layouts: none -> 10.6 us  [per_device(): jnp.split(jax.lax.all_gather(jnp.concatenate([packed_keys, values], 1), '...]
    dynamic_slice x24 -> x12, local copies, waits for them, and re-layouts: 15.5 us -> 15.3 us  [one_block(): lax.dynamic_slice_in_dim(value_piece, first, block, 0)]
  transfers between devices with their start and end apart: 4 -> 3, of which waited for: 4 -> 3; matrix products, arithmetic and copies ran while one was open for 6% -> 5% of each run, Pallas kernels for 0% -> 0%
where the time goes in v1:
time: 593 us; the launch traced here: 592 us
  matrix products  212 us (36%)
  waiting for transfers between devices  201 us (34%)
  other arithmetic  119 us (20%)
  local copies, waits for them, and re-layouts  34 us (6%)
  between operations  13.7 us (2%)
    all_gather x1, waiting for transfers between devices, per_device(): jax.lax.all_gather(jnp.concatenate([packed_keys, values], 1), 'sp', axis=...  145 us
    reduce_sum x12, other arithmetic, attend(): running_sum = running_sum * factor + jnp.sum(weights, axis=-1)  81.2 us
    dot_general x12, matrix products, attend(): jnp.einsum('hcqk,khe->hcqe', weights.astype(jnp.bfloat16), vals_blk, pref...  81.2 us
    dot_general x12, matrix products, attend(): jnp.einsum('qhcd,khcd->hcqk', query_rot, keys_blk, preferred_element_type...  80.2 us
    reduce_scatter x1, waiting for transfers between devices, per_device(): lax.psum_scatter(partial_value.astype(jnp.bfloat16), 'tp', scatter_dimens...  55.5 us
    dot_general x5, matrix products, project(): jnp.dot(hidden_states, weight, preferred_element_type=jnp.float32)  28.2 us
    add x12, other arithmetic, attend(): running_sum = running_sum * factor + jnp.sum(weights, axis=-1)  21.4 us
    dynamic_slice x12, local copies, waits for them, and re-layouts, one_block(): lax.dynamic_slice_in_dim(value_piece, first, block, 0)  15.3 us
  transfers between devices with their start and end apart: 3, of which 3 were waited for; matrix products, arithmetic and copies ran while one was open for 5% of the time, Pallas kernels for 0%

profile of v1, /device:TPU:0, one launch (start us, length us, event | category | flops | bytes accessed | tf_op | source)
XLA Modules:
  0.0 592.1 jit_solution(9650800619546742597)
XLA Ops:
  6.6 7.6 %convolution_convert_fusion = bf16[768,512]{0,1:T(8,128)(2,1)S(1)} fusion(bf16[768,4096]{1,0:T(8,128)(2,1)} %param.17, bf16[4096,512]{1,0:T(8,128)(2,1)} %param.22), kind=kOutput, calls=%fused_computation.57 | convolution fusion | flops 3221618688 | bytes 11272192 | tf_op jit(solution)/shard_map/dot_general | solution.py:52
  30.8 7.6 %convolution_convert_fusion.3 = bf16[768,512]{1,0:T(8,128)(2,1)S(1)} fusion(bf16[768,4096]{1,0:T(8,128)(2,1)} %param.17, bf16[4096,512]{1,0:T(8,128)(2,1)} %param.20), kind=kOutput, calls=%fused_computation.61 | convolution fusion | flops 3221618688 | bytes 11272192 | tf_op jit(solution)/shard_map/dot_general | solution.py:52
  50.5 14.2 %fusion.33 = f32[768,4096]{1,0:T(8,128)} fusion(bf16[512,4096]{1,0:T(8,128)(2,1)} %param.27, f32[2,512]{1,0:T(2,128)S(1)} %collective-permute-done, f32[768,512]{1,0:T(8,128)S(1)} %convert_multiply_fusion.1, bf16[768,4096]{1,0:T(8,128)(2,1)} %param.17, bf16[4096,512]{1,0:T(8,128)(2,1)} %param.18, f32[512]{0:T(512)S(1)} %bitcast.103, f32[512]{0:T(512)S(1)} %bitcast.102, ...), kind=kOutput, calls=%fused_computation.66 | convolution fusion | flops 6446776320 | bytes 28846080 | tf_op jit(solution)/shard_map/dot_general | solution.py:138
  64.7 144.5 %all-gather.2.cloned.1.call-done = bf16[6144,1024]{0,1:T(8,128)(2,1)} async-done(((bf16[768,1024]{0,1:T(8,128)(2,1)}), bf16[6144,1024]{0,1:T(8,128)(2,1)}) %all-gather.2.cloned.1.call-update) | async-done | bytes 12582928 | tf_op jit(solution)/shard_map/all_gather | solution.py:93
  209.3 295.2 %conditional.1 = (f32[4,2,768]{2,1,0:T(2,128)}, f32[4,2,768,128]{3,2,1,0:T(8,128)}) conditional(s32[]{:T(128)} %convert_element_type.98, () %tuple.27, (bf16[6144,1024]{0,1:T(8,128)(2,1)}, s32[]{:T(128)}, s32[768]{0:T(1024)S(1)}, bf16[768,4,2,64]{0,3,2,1:T(8,128)(2,1)S(1)}) %tuple.28), branch_computations={%region_0.0_spmd, %region_1.6_spmd} | conditional | flops 1251638528 | bytes 125449552 | solution.py:113
  209.3 10.6 %fusion.38 = (bf16[6144,512]{0,1:T(8,128)(2,1)}, bf16[6144,512]{0,1:T(8,128)(2,1)}) fusion(bf16[6144,1024]{0,1:T(8,128)(2,1)} %get-tuple-element.158), kind=kLoop, calls=%fused_computation.80 | loop fusion | bytes 25165824 | tf_op jit(solution)/shard_map/split | solution.py:92
  219.9 284.6 %while.17 = (s32[]{:T(128)}, f32[4,2,768]{2,1,0:T(2,128)S(1)}, f32[4,2,768]{2,1,0:T(2,128)}, f32[4,2,768,128]{3,2,1,0:T(8,128)}, s32[768]{0:T(1024)S(1)}, /*inde...) while((s32[]{:T(128)}, f32[4,2,768]{2,1,0:T(2,128)S(1)}, ...), condition=%wide.region_5.5_spmd.clone, body=%wide.region_2.4_spmd.clone.sunk | while | flops 1251637760 | bytes 100277456 | solution.py:111
  228.2 6.8 %fusion.74 = f32[4,2,768]{2,1,0:T(2,128)S(1)} fusion(f32[4,2,512,768]{3,2,1,0:T(8,128)} %get-tuple-element.298, f32[4,2,768]{2,1,0:T(2,128)S(1)} %fusion.73, pred[768,512]{0,1:T(8,128)(4,1)S(1)} %broadcast_compare_fusion.2), kind=kLoop, calls=%fused_computation.4.clone.1 | loop fusion | flops 15722496 | bytes 13025280 | tf_op jit(solution)/shard_map/cond/branch_1_fun/while/body/eval_jaxpr/reduce_sum | solution.py:77
  250.5 6.8 %fusion.74 = f32[4,2,768]{2,1,0:T(2,128)S(1)} fusion(f32[4,2,512,768]{3,2,1,0:T(8,128)} %get-tuple-element.298, f32[4,2,768]{2,1,0:T(2,128)S(1)} %fusion.73, pred[768,512]{0,1:T(8,128)(4,1)S(1)} %broadcast_compare_fusion.2), kind=kLoop, calls=%fused_computation.4.clone.1 | loop fusion | flops 15722496 | bytes 13025280 | tf_op jit(solution)/shard_map/cond/branch_1_fun/while/body/eval_jaxpr/reduce_sum | solution.py:77
  259.1 6.9 %fusion.76 = f32[4,2,768,128]{3,2,1,0:T(8,128)} fusion(f32[4,2,768,128]{3,2,1,0:T(8,128)} %get-tuple-element.317, bf16[512,4,128,1]{0,2,3,1:T(8,128)(2,1)S(1)} %bitcast.93, f32[4,2,512,768]{3,2,1,0:T(8,128)S(1)} %copy-done, f32[4,2,768]{2,1,0:T(2,128)S(1)} %fusion.73, pred[768,512]{0,1:T(8,128)(4,1)S(1)} %broadcast_compare_fusion.2, ...), kind=kOutput, calls=%fused_computation.8.clone.1 | convolution fusion | flops 823394304 | bytes 19841024 | tf_op jit(solution)/shard_map/cond/branch_1_fun/while/body/eval_jaxpr/hcqk,khe->hcqe/dot_general | solution.py:78
  274.3 6.8 %fusion.74 = f32[4,2,768]{2,1,0:T(2,128)S(1)} fusion(f32[4,2,512,768]{3,2,1,0:T(8,128)} %get-tuple-element.298, f32[4,2,768]{2,1,0:T(2,128)S(1)} %fusion.73, pred[768,512]{0,1:T(8,128)(4,1)S(1)} %broadcast_compare_fusion.2), kind=kLoop, calls=%fused_computation.4.clone.1 | loop fusion | flops 15722496 | bytes 13025280 | tf_op jit(solution)/shard_map/cond/branch_1_fun/while/body/eval_jaxpr/reduce_sum | solution.py:77
  283.0 6.9 %fusion.76 = f32[4,2,768,128]{3,2,1,0:T(8,128)} fusion(f32[4,2,768,128]{3,2,1,0:T(8,128)} %get-tuple-element.317, bf16[512,4,128,1]{0,2,3,1:T(8,128)(2,1)S(1)} %bitcast.93, f32[4,2,512,768]{3,2,1,0:T(8,128)S(1)} %copy-done, f32[4,2,768]{2,1,0:T(2,128)S(1)} %fusion.73, pred[768,512]{0,1:T(8,128)(4,1)S(1)} %broadcast_compare_fusion.2, ...), kind=kOutput, calls=%fused_computation.8.clone.1 | convolution fusion | flops 823394304 | bytes 19841024 | tf_op jit(solution)/shard_map/cond/branch_1_fun/while/body/eval_jaxpr/hcqk,khe->hcqe/dot_general | solution.py:78
  298.2 6.8 %fusion.74 = f32[4,2,768]{2,1,0:T(2,128)S(1)} fusion(f32[4,2,512,768]{3,2,1,0:T(8,128)} %get-tuple-element.298, f32[4,2,768]{2,1,0:T(2,128)S(1)} %fusion.73, pred[768,512]{0,1:T(8,128)(4,1)S(1)} %broadcast_compare_fusion.2), kind=kLoop, calls=%fused_computation.4.clone.1 | loop fusion | flops 15722496 | bytes 13025280 | tf_op jit(solution)/shard_map/cond/branch_1_fun/while/body/eval_jaxpr/reduce_sum | solution.py:77
  306.8 6.9 %fusion.76 = f32[4,2,768,128]{3,2,1,0:T(8,128)} fusion(f32[4,2,768,128]{3,2,1,0:T(8,128)} %get-tuple-element.317, bf16[512,4,128,1]{0,2,3,1:T(8,128)(2,1)S(1)} %bitcast.93, f32[4,2,512,768]{3,2,1,0:T(8,128)S(1)} %copy-done, f32[4,2,768]{2,1,0:T(2,128)S(1)} %fusion.73, pred[768,512]{0,1:T(8,128)(4,1)S(1)} %broadcast_compare_fusion.2, ...), kind=kOutput, calls=%fused_computation.8.clone.1 | convolution fusion | flops 823394304 | bytes 19841024 | tf_op jit(solution)/shard_map/cond/branch_1_fun/while/body/eval_jaxpr/hcqk,khe->hcqe/dot_general | solution.py:78
  322.0 6.8 %fusion.74 = f32[4,2,768]{2,1,0:T(2,128)S(1)} fusion(f32[4,2,512,768]{3,2,1,0:T(8,128)} %get-tuple-element.298, f32[4,2,768]{2,1,0:T(2,128)S(1)} %fusion.73, pred[768,512]{0,1:T(8,128)(4,1)S(1)} %broadcast_compare_fusion.2), kind=kLoop, calls=%fused_computation.4.clone.1 | loop fusion | flops 15722496 | bytes 13025280 | tf_op jit(solution)/shard_map/cond/branch_1_fun/while/body/eval_jaxpr/reduce_sum | solution.py:77
  330.7 6.9 %fusion.76 = f32[4,2,768,128]{3,2,1,0:T(8,128)} fusion(f32[4,2,768,128]{3,2,1,0:T(8,128)} %get-tuple-element.317, bf16[512,4,128,1]{0,2,3,1:T(8,128)(2,1)S(1)} %bitcast.93, f32[4,2,512,768]{3,2,1,0:T(8,128)S(1)} %copy-done, f32[4,2,768]{2,1,0:T(2,128)S(1)} %fusion.73, pred[768,512]{0,1:T(8,128)(4,1)S(1)} %broadcast_compare_fusion.2, ...), kind=kOutput, calls=%fused_computation.8.clone.1 | convolution fusion | flops 823394304 | bytes 19841024 | tf_op jit(solution)/shard_map/cond/branch_1_fun/while/body/eval_jaxpr/hcqk,khe->hcqe/dot_general | solution.py:78
  345.9 6.8 %fusion.74 = f32[4,2,768]{2,1,0:T(2,128)S(1)} fusion(f32[4,2,512,768]{3,2,1,0:T(8,128)} %get-tuple-element.298, f32[4,2,768]{2,1,0:T(2,128)S(1)} %fusion.73, pred[768,512]{0,1:T(8,128)(4,1)S(1)} %broadcast_compare_fusion.2), kind=kLoop, calls=%fused_computation.4.clone.1 | loop fusion | flops 15722496 | bytes 13025280 | tf_op jit(solution)/shard_map/cond/branch_1_fun/while/body/eval_jaxpr/reduce_sum | solution.py:77
  354.5 6.9 %fusion.76 = f32[4,2,768,128]{3,2,1,0:T(8,128)} fusion(f32[4,2,768,128]{3,2,1,0:T(8,128)} %get-tuple-element.317, bf16[512,4,128,1]{0,2,3,1:T(8,128)(2,1)S(1)} %bitcast.93, f32[4,2,512,768]{3,2,1,0:T(8,128)S(1)} %copy-done, f32[4,2,768]{2,1,0:T(2,128)S(1)} %fusion.73, pred[768,512]{0,1:T(8,128)(4,1)S(1)} %broadcast_compare_fusion.2, ...), kind=kOutput, calls=%fused_computation.8.clone.1 | convolution fusion | flops 823394304 | bytes 19841024 | tf_op jit(solution)/shard_map/cond/branch_1_fun/while/body/eval_jaxpr/hcqk,khe->hcqe/dot_general | solution.py:78
  369.7 6.8 %fusion.74 = f32[4,2,768]{2,1,0:T(2,128)S(1)} fusion(f32[4,2,512,768]{3,2,1,0:T(8,128)} %get-tuple-element.298, f32[4,2,768]{2,1,0:T(2,128)S(1)} %fusion.73, pred[768,512]{0,1:T(8,128)(4,1)S(1)} %broadcast_compare_fusion.2), kind=kLoop, calls=%fused_computation.4.clone.1 | loop fusion | flops 15722496 | bytes 13025280 | tf_op jit(solution)/shard_map/cond/branch_1_fun/while/body/eval_jaxpr/reduce_sum | solution.py:77
  378.4 6.9 %fusion.76 = f32[4,2,768,128]{3,2,1,0:T(8,128)} fusion(f32[4,2,768,128]{3,2,1,0:T(8,128)} %get-tuple-element.317, bf16[512,4,128,1]{0,2,3,1:T(8,128)(2,1)S(1)} %bitcast.93, f32[4,2,512,768]{3,2,1,0:T(8,128)S(1)} %copy-done, f32[4,2,768]{2,1,0:T(2,128)S(1)} %fusion.73, pred[768,512]{0,1:T(8,128)(4,1)S(1)} %broadcast_compare_fusion.2, ...), kind=kOutput, calls=%fused_computation.8.clone.1 | convolution fusion | flops 823394304 | bytes 19841024 | tf_op jit(solution)/shard_map/cond/branch_1_fun/while/body/eval_jaxpr/hcqk,khe->hcqe/dot_general | solution.py:78
  393.6 6.8 %fusion.74 = f32[4,2,768]{2,1,0:T(2,128)S(1)} fusion(f32[4,2,512,768]{3,2,1,0:T(8,128)} %get-tuple-element.298, f32[4,2,768]{2,1,0:T(2,128)S(1)} %fusion.73, pred[768,512]{0,1:T(8,128)(4,1)S(1)} %broadcast_compare_fusion.2), kind=kLoop, calls=%fused_computation.4.clone.1 | loop fusion | flops 15722496 | bytes 13025280 | tf_op jit(solution)/shard_map/cond/branch_1_fun/while/body/eval_jaxpr/reduce_sum | solution.py:77
  402.2 6.9 %fusion.76 = f32[4,2,768,128]{3,2,1,0:T(8,128)} fusion(f32[4,2,768,128]{3,2,1,0:T(8,128)} %get-tuple-element.317, bf16[512,4,128,1]{0,2,3,1:T(8,128)(2,1)S(1)} %bitcast.93, f32[4,2,512,768]{3,2,1,0:T(8,128)S(1)} %copy-done, f32[4,2,768]{2,1,0:T(2,128)S(1)} %fusion.73, pred[768,512]{0,1:T(8,128)(4,1)S(1)} %broadcast_compare_fusion.2, ...), kind=kOutput, calls=%fused_computation.8.clone.1 | convolution fusion | flops 823394304 | bytes 19841024 | tf_op jit(solution)/shard_map/cond/branch_1_fun/while/body/eval_jaxpr/hcqk,khe->hcqe/dot_general | solution.py:78
  417.4 6.8 %fusion.74 = f32[4,2,768]{2,1,0:T(2,128)S(1)} fusion(f32[4,2,512,768]{3,2,1,0:T(8,128)} %get-tuple-element.298, f32[4,2,768]{2,1,0:T(2,128)S(1)} %fusion.73, pred[768,512]{0,1:T(8,128)(4,1)S(1)} %broadcast_compare_fusion.2), kind=kLoop, calls=%fused_computation.4.clone.1 | loop fusion | flops 15722496 | bytes 13025280 | tf_op jit(solution)/shard_map/cond/branch_1_fun/while/body/eval_jaxpr/reduce_sum | solution.py:77
  426.1 6.9 %fusion.76 = f32[4,2,768,128]{3,2,1,0:T(8,128)} fusion(f32[4,2,768,128]{3,2,1,0:T(8,128)} %get-tuple-element.317, bf16[512,4,128,1]{0,2,3,1:T(8,128)(2,1)S(1)} %bitcast.93, f32[4,2,512,768]{3,2,1,0:T(8,128)S(1)} %copy-done, f32[4,2,768]{2,1,0:T(2,128)S(1)} %fusion.73, pred[768,512]{0,1:T(8,128)(4,1)S(1)} %broadcast_compare_fusion.2, ...), kind=kOutput, calls=%fused_computation.8.clone.1 | convolution fusion | flops 823394304 | bytes 19841024 | tf_op jit(solution)/shard_map/cond/branch_1_fun/while/body/eval_jaxpr/hcqk,khe->hcqe/dot_general | solution.py:78
  441.2 6.8 %fusion.74 = f32[4,2,768]{2,1,0:T(2,128)S(1)} fusion(f32[4,2,512,768]{3,2,1,0:T(8,128)} %get-tuple-element.298, f32[4,2,768]{2,1,0:T(2,128)S(1)} %fusion.73, pred[768,512]{0,1:T(8,128)(4,1)S(1)} %broadcast_compare_fusion.2), kind=kLoop, calls=%fused_computation.4.clone.1 | loop fusion | flops 15722496 | bytes 13025280 | tf_op jit(solution)/shard_map/cond/branch_1_fun/while/body/eval_jaxpr/reduce_sum | solution.py:77
  449.9 6.9 %fusion.76 = f32[4,2,768,128]{3,2,1,0:T(8,128)} fusion(f32[4,2,768,128]{3,2,1,0:T(8,128)} %get-tuple-element.317, bf16[512,4,128,1]{0,2,3,1:T(8,128)(2,1)S(1)} %bitcast.93, f32[4,2,512,768]{3,2,1,0:T(8,128)S(1)} %copy-done, f32[4,2,768]{2,1,0:T(2,128)S(1)} %fusion.73, pred[768,512]{0,1:T(8,128)(4,1)S(1)} %broadcast_compare_fusion.2, ...), kind=kOutput, calls=%fused_computation.8.clone.1 | convolution fusion | flops 823394304 | bytes 19841024 | tf_op jit(solution)/shard_map/cond/branch_1_fun/while/body/eval_jaxpr/hcqk,khe->hcqe/dot_general | solution.py:78
  465.1 6.8 %fusion.74 = f32[4,2,768]{2,1,0:T(2,128)S(1)} fusion(f32[4,2,512,768]{3,2,1,0:T(8,128)} %get-tuple-element.298, f32[4,2,768]{2,1,0:T(2,128)S(1)} %fusion.73, pred[768,512]{0,1:T(8,128)(4,1)S(1)} %broadcast_compare_fusion.2), kind=kLoop, calls=%fused_computation.4.clone.1 | loop fusion | flops 15722496 | bytes 13025280 | tf_op jit(solution)/shard_map/cond/branch_1_fun/while/body/eval_jaxpr/reduce_sum | solution.py:77
  473.7 6.9 %fusion.76 = f32[4,2,768,128]{3,2,1,0:T(8,128)} fusion(f32[4,2,768,128]{3,2,1,0:T(8,128)} %get-tuple-element.317, bf16[512,4,128,1]{0,2,3,1:T(8,128)(2,1)S(1)} %bitcast.93, f32[4,2,512,768]{3,2,1,0:T(8,128)S(1)} %copy-done, f32[4,2,768]{2,1,0:T(2,128)S(1)} %fusion.73, pred[768,512]{0,1:T(8,128)(4,1)S(1)} %broadcast_compare_fusion.2, ...), kind=kOutput, calls=%fused_computation.8.clone.1 | convolution fusion | flops 823394304 | bytes 19841024 | tf_op jit(solution)/shard_map/cond/branch_1_fun/while/body/eval_jaxpr/hcqk,khe->hcqe/dot_general | solution.py:78
  488.9 6.8 %fusion.74 = f32[4,2,768]{2,1,0:T(2,128)S(1)} fusion(f32[4,2,512,768]{3,2,1,0:T(8,128)} %get-tuple-element.298, f32[4,2,768]{2,1,0:T(2,128)S(1)} %fusion.73, pred[768,512]{0,1:T(8,128)(4,1)S(1)} %broadcast_compare_fusion.2), kind=kLoop, calls=%fused_computation.4.clone.1 | loop fusion | flops 15722496 | bytes 13025280 | tf_op jit(solution)/shard_map/cond/branch_1_fun/while/body/eval_jaxpr/reduce_sum | solution.py:77
  497.6 6.9 %fusion.76 = f32[4,2,768,128]{3,2,1,0:T(8,128)} fusion(f32[4,2,768,128]{3,2,1,0:T(8,128)} %get-tuple-element.317, bf16[512,4,128,1]{0,2,3,1:T(8,128)(2,1)S(1)} %bitcast.93, f32[4,2,512,768]{3,2,1,0:T(8,128)S(1)} %copy-done, f32[4,2,768]{2,1,0:T(2,128)S(1)} %fusion.73, pred[768,512]{0,1:T(8,128)(4,1)S(1)} %broadcast_compare_fusion.2, ...), kind=kOutput, calls=%fused_computation.8.clone.1 | convolution fusion | flops 823394304 | bytes 19841024 | tf_op jit(solution)/shard_map/cond/branch_1_fun/while/body/eval_jaxpr/hcqk,khe->hcqe/dot_general | solution.py:78
  509.9 8.2 %add_convert_fusion = bf16[768,4096]{1,0:T(8,128)(2,1)} fusion(f32[768,4096]{1,0:T(8,128)} %fusion.33, bf16[768,512]{0,1:T(8,128)(2,1)S(1)} %bitcast.98, bf16[512,4096]{1,0:T(8,128)(2,1)S(1)} %copy-done.7), kind=kOutput, calls=%fused_computation.22 | convolution fusion | flops 3227516928 | bytes 23855104 | tf_op jit(solution)/shard_map/dot_general | solution.py:138
  518.9 55.5 %reduce-scatter.2.cloned.1.call-done = bf16[768,1024]{1,0:T(8,128)(2,1)} async-done(((bf16[768,4096]{1,0:T(8,128)(2,1)}), bf16[768,1024]{1,0:T(8,128)(2,1)}) %reduce-scatter.2.cloned.1.call-update) | async-done | bytes 1572880 | tf_op jit(solution)/shard_map/reduce_scatter | solution.py:141
  (169 shorter events, 172.8 us)
Async XLA Ops:
  6.5 202.7 %all-gather.2.cloned.1.call-start = ((), (), s32[]{:S(2)}) async-start(), calls=%async_computation.1 | async-start | bytes 14155776 | tf_op jit(solution)/shard_map/all_gather | solution.py:93
  6.5 9.9 %copy-start.3 = (bf16[768,4096]{1,0:T(8,128)(2,1)S(1)}, bf16[768,4096]{1,0:T(8,128)(2,1)}, u32[]{:S(2)}) copy-start(bf16[768,4096]{1,0:T(8,128)(2,1)} %param.17) | copy-start | bytes 18874372
  6.6 9.9 %copy-start.4 = (bf16[4096,512]{1,0:T(8,128)(2,1)S(1)}, bf16[4096,512]{1,0:T(8,128)(2,1)}, u32[]{:S(2)}) copy-start(bf16[4096,512]{1,0:T(8,128)(2,1)} %param.23) | copy-start | bytes 12582916
  20.7 3.4 slice-start
  22.2 2.1 slice-start.1
  22.2 3.2 copy-start.5
  30.5 543.9 %reduce-scatter.2.cloned.1.call-start = ((), (), s32[]{:S(2)}) async-start(), calls=%async_computation.2 | async-start | bytes 7864320 | tf_op jit(solution)/shard_map/reduce_scatter | solution.py:141
  30.8 7.6 %copy-start.6 = (bf16[4096,512]{1,0:T(8,128)(2,1)S(1)}, bf16[4096,512]{1,0:T(8,128)(2,1)}, u32[]{:S(2)}) copy-start(bf16[4096,512]{1,0:T(8,128)(2,1)} %param.19) | copy-start | bytes 12582916
  38.3 10.9 %copy-start.1 = (bf16[3,512]{1,0:T(4,128)(2,1)S(1)}, bf16[3,512]{1,0:T(4,128)(2,1)}, u32[]{:S(2)}) copy-start(bf16[3,512]{1,0:T(4,128)(2,1)} %param.21) | copy-start | bytes 9220
  38.3 10.9 %copy-start.8 = (bf16[128]{0:T(256)(128)(2,1)S(1)}, bf16[128]{0:T(256)(128)(2,1)}, u32[]{:S(2)}) copy-start(bf16[128]{0:T(256)(128)(2,1)} %param.26) | copy-start | bytes 772
  43.9 6.7 %collective-permute-start = (f32[2,512]{1,0:T(2,128)S(1)}, f32[2,512]{1,0:T(2,128)S(1)}, u32[]{:S(2)}, u32[]{:S(2)}) collective-permute-start(f32[2,512]{1,0:T(2,128)S(1)} %slice.41), channel_id=1, source_target_pairs={{0,4},{4,8},{8,12},{12,16},{16,20},{20,24},{24,28},{1,5},{5,9},{9,... | collective-permute-start | bytes 12296 | tf_op jit(solution)/shard_map/ppermute | solution.py:16
  228.2 8.3 %copy-start = (f32[4,2,512,768]{3,2,1,0:T(8,128)S(1)}, f32[4,2,512,768]{3,2,1,0:T(8,128)}, u32[]{:S(2)}) copy-start(f32[4,2,512,768]{3,2,1,0:T(8,128)} %get-tuple-element.298) | copy-start | bytes 37748740 | tf_op jit(solution)/shard_map/cond/branch_1_fun/while
  250.5 8.7 %copy-start = (f32[4,2,512,768]{3,2,1,0:T(8,128)S(1)}, f32[4,2,512,768]{3,2,1,0:T(8,128)}, u32[]{:S(2)}) copy-start(f32[4,2,512,768]{3,2,1,0:T(8,128)} %get-tuple-element.298) | copy-start | bytes 37748740 | tf_op jit(solution)/shard_map/cond/branch_1_fun/while
  274.3 8.7 %copy-start = (f32[4,2,512,768]{3,2,1,0:T(8,128)S(1)}, f32[4,2,512,768]{3,2,1,0:T(8,128)}, u32[]{:S(2)}) copy-start(f32[4,2,512,768]{3,2,1,0:T(8,128)} %get-tuple-element.298) | copy-start | bytes 37748740 | tf_op jit(solution)/shard_map/cond/branch_1_fun/while
  298.2 8.7 %copy-start = (f32[4,2,512,768]{3,2,1,0:T(8,128)S(1)}, f32[4,2,512,768]{3,2,1,0:T(8,128)}, u32[]{:S(2)}) copy-start(f32[4,2,512,768]{3,2,1,0:T(8,128)} %get-tuple-element.298) | copy-start | bytes 37748740 | tf_op jit(solution)/shard_map/cond/branch_1_fun/while
  322.0 8.7 %copy-start = (f32[4,2,512,768]{3,2,1,0:T(8,128)S(1)}, f32[4,2,512,768]{3,2,1,0:T(8,128)}, u32[]{:S(2)}) copy-start(f32[4,2,512,768]{3,2,1,0:T(8,128)} %get-tuple-element.298) | copy-start | bytes 37748740 | tf_op jit(solution)/shard_map/cond/branch_1_fun/while
  345.9 8.7 %copy-start = (f32[4,2,512,768]{3,2,1,0:T(8,128)S(1)}, f32[4,2,512,768]{3,2,1,0:T(8,128)}, u32[]{:S(2)}) copy-start(f32[4,2,512,768]{3,2,1,0:T(8,128)} %get-tuple-element.298) | copy-start | bytes 37748740 | tf_op jit(solution)/shard_map/cond/branch_1_fun/while
  369.7 8.7 %copy-start = (f32[4,2,512,768]{3,2,1,0:T(8,128)S(1)}, f32[4,2,512,768]{3,2,1,0:T(8,128)}, u32[]{:S(2)}) copy-start(f32[4,2,512,768]{3,2,1,0:T(8,128)} %get-tuple-element.298) | copy-start | bytes 37748740 | tf_op jit(solution)/shard_map/cond/branch_1_fun/while
  393.6 8.7 %copy-start = (f32[4,2,512,768]{3,2,1,0:T(8,128)S(1)}, f32[4,2,512,768]{3,2,1,0:T(8,128)}, u32[]{:S(2)}) copy-start(f32[4,2,512,768]{3,2,1,0:T(8,128)} %get-tuple-element.298) | copy-start | bytes 37748740 | tf_op jit(solution)/shard_map/cond/branch_1_fun/while
  417.4 8.7 %copy-start = (f32[4,2,512,768]{3,2,1,0:T(8,128)S(1)}, f32[4,2,512,768]{3,2,1,0:T(8,128)}, u32[]{:S(2)}) copy-start(f32[4,2,512,768]{3,2,1,0:T(8,128)} %get-tuple-element.298) | copy-start | bytes 37748740 | tf_op jit(solution)/shard_map/cond/branch_1_fun/while
  441.2 8.7 %copy-start = (f32[4,2,512,768]{3,2,1,0:T(8,128)S(1)}, f32[4,2,512,768]{3,2,1,0:T(8,128)}, u32[]{:S(2)}) copy-start(f32[4,2,512,768]{3,2,1,0:T(8,128)} %get-tuple-element.298) | copy-start | bytes 37748740 | tf_op jit(solution)/shard_map/cond/branch_1_fun/while
  465.1 8.7 %copy-start = (f32[4,2,512,768]{3,2,1,0:T(8,128)S(1)}, f32[4,2,512,768]{3,2,1,0:T(8,128)}, u32[]{:S(2)}) copy-start(f32[4,2,512,768]{3,2,1,0:T(8,128)} %get-tuple-element.298) | copy-start | bytes 37748740 | tf_op jit(solution)/shard_map/cond/branch_1_fun/while
  488.9 8.7 %copy-start = (f32[4,2,512,768]{3,2,1,0:T(8,128)S(1)}, f32[4,2,512,768]{3,2,1,0:T(8,128)}, u32[]{:S(2)}) copy-start(f32[4,2,512,768]{3,2,1,0:T(8,128)} %get-tuple-element.298) | copy-start | bytes 37748740 | tf_op jit(solution)/shard_map/cond/branch_1_fun/while
  505.3 2.4 copy-start.2
  507.7 2.2 copy-start.7
Sparse Core Ops, SparseCore 0:
  30.6 178.5 all-gather.1
  518.3 56.0 reduce-scatter.1
